TPU v7x, 32 devices: a whole 2x2x4 slice. The times are simulated.
32 devices in a mesh: ep: 4 (over z), tp: 8 (over y, x, core).
Axes of the slice: x: 2, y: 2, z: 4, core: 2. Of those that a mesh axis runs over, the one named last changes fastest.
Arguments:
- tokens: bfloat16 [32, 4096], P('ep'), may hold values from -6 to 6
- norm_gains: float32 [4, 4096], replicated, may hold values from 0.1 to 1.9
- w_query: bfloat16 [4096, 4096], P(None, 'tp'), may hold values from -0.09375 to 0.09375
- w_query_rope: bfloat16 [4096, 2048], P(None, 'tp'), may hold values from -0.09375 to 0.09375
- w_key_up: bfloat16 [32, 128, 1024], P('tp'), may hold values from -0.5 to 0.5
- w_value_up: bfloat16 [32, 1024, 128], P('tp'), may hold values from -0.1875 to 0.1875
- w_output: bfloat16 [4096, 4096], P('tp'), may hold values from -0.09375 to 0.09375
- w_latent_down: bfloat16 [4096, 1024], P(None, 'tp'), may hold values from -0.09375 to 0.09375
- latent_gain: float32 [1024], replicated, may hold values from 0.1 to 1.9
- w_rope_down: bfloat16 [4096, 64], replicated, may hold values from -0.09375 to 0.09375
- cache_latent: bfloat16 [32, 1024, 1024], P(('ep', 'tp')), may hold values from -300 to 300
- cache_rope: bfloat16 [32, 1024, 64], P(('ep', 'tp')), may hold values from -6 to 6
- lengths: int32 [32], P(('ep', 'tp')), may hold values from 1 to 1024, as said below
- routes: int32 [32, 2], P('ep'), may hold values from 0 to 3, all different within a row; in each aligned block of 8 rows (0 to 7, 8 to 15, ...) at most 7 rows name the same one
- route_weights: float32 [32, 2], P('ep'), may hold values from 0.2 to 1
- w_gate: bfloat16 [4, 4096, 2048], P('ep', None, 'tp'), may hold values from -0.09375 to 0.09375
- w_up: bfloat16 [4, 4096, 2048], P('ep', None, 'tp'), may hold values from -0.09375 to 0.09375
- w_down: bfloat16 [4, 2048, 4096], P('ep', 'tp'), may hold values from -0.125 to 0.125
Outputs:
- hidden_out: bfloat16 [32, 4096], P(('ep', 'tp'))
- new_latent: bfloat16 [32, 1024], P(('ep', 'tp'))
- new_rope: bfloat16 [32, 64], P(('ep', 'tp'))
Inputs may be any that keep to these rules, and one draw needn't show every extreme that they name: `routes`: within each aligned block of 8 rows no expert is named by more than 7 rows, a bound that some block reaches; the 2 experts of a row differ. The new token stands at position lengths; some sequence has exactly 1024.
All inputs are finite; a program needn't handle non-finite values.
Results may differ from a plain program's by a relative error of at most 0.02.
Values may be sent and summed in bfloat16 or wider, within the bound.
A program may use at most 64 MiB of HBM per device.

v0:
```python
import jax
import jax.numpy as jnp
from jax import lax
from jax.sharding import PartitionSpec as P

EXP_LOCAL = 1
EPSILON = 1e-06
ROTARY_BASE = 500000.0


def rms_scale(source, gain_row):
    values_f = source.astype(jnp.float32)
    return (
        values_f
        * lax.rsqrt(jnp.mean(values_f * values_f, axis=-1, keepdims=True) + EPSILON)
        * gain_row
    )


def rotate(source, position):
    half_width = source.shape[-1] // 2
    frequency = ROTARY_BASE ** (-jnp.arange(half_width, dtype=jnp.float32) / half_width)
    angles = position[..., None] * frequency
    first_half = source[..., :half_width]
    second_half = source[..., half_width:]
    return jnp.concatenate(
        [
            first_half * jnp.cos(angles) - second_half * jnp.sin(angles),
            second_half * jnp.cos(angles) + first_half * jnp.sin(angles),
        ],
        axis=-1,
    )


def attend(q_latent, q_pe, cache_lat, cache_rp, lat_new, rope_new, lengths, score_scale):
    scores = (
        jnp.einsum("shc,spc->shp", q_latent, cache_lat, preferred_element_type=jnp.float32)
        + jnp.einsum("shr,spr->shp", q_pe, cache_rp, preferred_element_type=jnp.float32)
    ) * score_scale
    own_score = (
        jnp.einsum("shc,sc->sh", q_latent, lat_new, preferred_element_type=jnp.float32)
        + jnp.einsum("shr,sr->sh", q_pe, rope_new, preferred_element_type=jnp.float32)
    ) * score_scale
    visible = (
        jnp.arange(cache_lat.shape[1], dtype=jnp.int32)[None, None, :] < lengths[:, None, None]
    )
    row_max = jnp.maximum(jnp.max(jnp.where(visible, scores, -jnp.inf), axis=-1), own_score)
    weights = jnp.where(visible, jnp.exp(scores - row_max[..., None]), 0.0)
    own_weight = jnp.exp(own_score - row_max)
    denominator = jnp.sum(weights, axis=-1) + own_weight
    probabilities = (weights / denominator[..., None]).astype(jnp.bfloat16)
    own_prob = (own_weight / denominator).astype(jnp.bfloat16)
    attended = jnp.einsum(
        "shp,spc->shc", probabilities, cache_lat, preferred_element_type=jnp.float32
    )
    attended = (
        attended + own_prob.astype(jnp.float32)[..., None] * lat_new.astype(jnp.float32)[:, None, :]
    )
    return attended.astype(jnp.bfloat16)


def on_device(
    tokens,
    norm_gains,
    w_query,
    w_query_rope,
    w_key_up,
    w_value_up,
    w_output,
    w_latent_down,
    latent_gain,
    w_rope_down,
    cache_latent,
    cache_rope,
    lengths,
    routes,
    route_weights,
    w_gate,
    w_up,
    w_down,
):
    group_rows = tokens.shape[0]
    seq_count = cache_latent.shape[0]
    heads_here = w_key_up.shape[0]
    nope_width = w_key_up.shape[1]
    rope_width = w_rope_down.shape[1]
    tp_size = lax.axis_size("tp")
    tp_rank = lax.axis_index("tp")
    normed = rms_scale(tokens, norm_gains[0]).astype(jnp.bfloat16)
    q_nope = jnp.dot(normed, w_query, preferred_element_type=jnp.float32).astype(jnp.bfloat16)
    q_nope = q_nope.reshape(group_rows, heads_here, nope_width)
    q_latent = jnp.einsum("thn,hnc->thc", q_nope, w_key_up, preferred_element_type=jnp.float32)
    q_latent = q_latent.astype(jnp.bfloat16).reshape(group_rows, -1)
    q_rot = jnp.dot(normed, w_query_rope, preferred_element_type=jnp.float32).astype(jnp.bfloat16)
    latent_cols = jnp.dot(normed, w_latent_down, preferred_element_type=jnp.float32).astype(
        jnp.bfloat16
    )
    q_mine, rot_mine, latent_raw = (
        lax.all_to_all(q_latent, "tp", split_axis=0, concat_axis=1, tiled=True),
        lax.all_to_all(q_rot, "tp", split_axis=0, concat_axis=1, tiled=True),
        lax.all_to_all(latent_cols, "tp", split_axis=0, concat_axis=1, tiled=True),
    )
    heads_all = rot_mine.shape[1] // rope_width
    own_normed = lax.dynamic_slice_in_dim(normed, tp_rank * seq_count, seq_count, 0)
    rope_raw = jnp.dot(own_normed, w_rope_down, preferred_element_type=jnp.float32).astype(
        jnp.bfloat16
    )
    new_latent = rms_scale(latent_raw, latent_gain).astype(jnp.bfloat16)
    position = lengths.astype(jnp.float32)
    new_rope = rotate(rope_raw.astype(jnp.float32), position).astype(jnp.bfloat16)
    q_pe = rotate(
        rot_mine.reshape(seq_count, heads_all, rope_width).astype(jnp.float32), position[:, None]
    )
    q_pe = q_pe.astype(jnp.bfloat16)
    score_scale = (nope_width + rope_width) ** (-0.5)
    attended = attend(
        q_mine.reshape(seq_count, heads_all, -1),
        q_pe,
        cache_latent,
        cache_rope,
        new_latent,
        new_rope,
        lengths,
        score_scale,
    )
    head_latent = lax.all_to_all(
        attended.reshape(seq_count, -1), "tp", split_axis=1, concat_axis=0, tiled=True
    )
    values = (
        jnp.einsum(
            "thc,hcv->thv",
            head_latent.reshape(group_rows, heads_here, -1),
            w_value_up,
            preferred_element_type=jnp.float32,
        )
        .astype(jnp.bfloat16)
        .reshape(group_rows, -1)
    )
    head_term = jnp.dot(values, w_output, preferred_element_type=jnp.float32)
    mixed = lax.psum(head_term.astype(jnp.bfloat16), "tp").astype(jnp.float32)
    resid = (tokens.astype(jnp.float32) + rms_scale(mixed, norm_gains[1])).astype(jnp.bfloat16)
    expert_in = rms_scale(resid, norm_gains[2]).astype(jnp.bfloat16)
    own_resid = lax.dynamic_slice_in_dim(resid, tp_rank * seq_count, seq_count, 0)
    ep_size = lax.axis_size("ep")
    experts = ep_size * EXP_LOCAL
    local_expert = tp_rank // (tp_size // EXP_LOCAL)
    route_count = routes.shape[1]
    capacity = (
        (group_rows * route_count + experts - 1) // experts
        + 2
        + group_rows * route_count // (4 * experts)
    )
    slot_count = ep_size * capacity
    flat_routes = routes.reshape(-1)
    expert_hits = (flat_routes[:, None] == jnp.arange(experts, dtype=jnp.int32)[None, :]).astype(
        jnp.int32
    )
    slot_rank = jnp.sum((jnp.cumsum(expert_hits, axis=0) - 1) * expert_hits, axis=1)
    served_here = flat_routes % EXP_LOCAL == local_expert
    slot_index = jnp.where(served_here, flat_routes // EXP_LOCAL * capacity + slot_rank, -1)
    slot_picks = (slot_index[:, None] == jnp.arange(slot_count, dtype=jnp.int32)[None, :]).astype(
        jnp.bfloat16
    )
    slot_picks = slot_picks.reshape(group_rows, route_count, slot_count)
    slot_rows = jnp.sum(slot_picks, axis=1)
    outgoing = jnp.dot(slot_rows.T, expert_in, preferred_element_type=jnp.float32).astype(
        jnp.bfloat16
    )
    arrived = lax.all_to_all(outgoing, "ep", split_axis=0, concat_axis=0, tiled=True)
    gate_sum = jnp.dot(arrived, w_gate[0], preferred_element_type=jnp.float32)
    up_sum = jnp.dot(arrived, w_up[0], preferred_element_type=jnp.float32)
    hidden_units = (jax.nn.silu(gate_sum) * up_sum).astype(jnp.bfloat16)
    expert_out = jnp.dot(hidden_units, w_down[0], preferred_element_type=jnp.float32).astype(
        jnp.bfloat16
    )
    returned = lax.all_to_all(expert_out, "ep", split_axis=0, concat_axis=0, tiled=True)
    routed_part = jnp.zeros((group_rows, returned.shape[1]), jnp.float32)
    for route_slot in range(route_count):
        chosen = jnp.dot(slot_picks[:, route_slot, :], returned, preferred_element_type=jnp.float32)
        routed_part = routed_part + route_weights[:, route_slot : route_slot + 1] * chosen
    routed = lax.psum_scatter(
        routed_part.astype(jnp.bfloat16), "tp", scatter_dimension=0, tiled=True
    ).astype(jnp.float32)
    hidden_out = (own_resid.astype(jnp.float32) + rms_scale(routed, norm_gains[3])).astype(
        jnp.bfloat16
    )
    return (hidden_out, new_latent, new_rope)


def solution(mesh):
    in_specs = (
        P("ep", None),
        P(),
        P(None, "tp"),
        P(None, "tp"),
        P("tp", None, None),
        P("tp", None, None),
        P("tp", None),
        P(None, "tp"),
        P(),
        P(),
        P(("ep", "tp"), None, None),
        P(("ep", "tp"), None, None),
        P(("ep", "tp")),
        P("ep", None),
        P("ep", None),
        P("ep", None, "tp"),
        P("ep", None, "tp"),
        P("ep", "tp", None),
    )
    out_specs = (P(("ep", "tp"), None), P(("ep", "tp"), None), P(("ep", "tp"), None))
    return jax.shard_map(
        on_device, mesh=mesh, in_specs=in_specs, out_specs=out_specs, check_vma=False
    )
```

profile of v0, /device:TPU:0, one launch (start us, length us, event | category | flops | bytes accessed | tf_op | source)
XLA Modules:
  0.0 212.2 jit_solution(539098069489857588)
XLA Ops:
  7.2 1.1 fusion.78
  8.3 1.0 fusion.40
  9.3 0.9 fusion.42
  10.2 1.5 fusion.29
  11.7 0.6 copy.35
  12.3 5.2 %all-to-all-start.2 = ((bf16[8,1,128]{2,1,0:T(2,128)(2,1)}), bf16[8,1,128]{2,1,0:T(2,128)(2,1)S(1)}, u32[]{:S(2)}, u32[]{:S(2)}) async-start(bf16[8,1,128]{2,1,0:T(2,128)(2,1)} %copy.35), calls=%async_computation.2 | async-start | bytes 8192 | tf_op jit(solution)/shard_map/all_to_all | solution.py:101
  17.5 2.0 fusion.28
  20.2 1.3 fusion.34
  22.1 3.1 %convolution_convert_fusion.3 = bf16[4,8,1024]{2,1,0:T(8,128)(2,1)S(1)} fusion(bf16[4,128,1024]{2,1,0:T(8,128)(2,1)S(1)} %copy-done.2, bf16[8,4096]{1,0:T(8,128)(2,1)S(1)} %fusion.42, bf16[4096,512]{1,0:T(8,128)(2,1)} %param.20), kind=kOutput, calls=%fused_computation.20 | convolution fusion | flops 41979904 | bytes 5373952 | tf_op jit(solution)/shard_map/thn,hnc->thc/dot_general | solution.py:92
  25.1 0.5 broadcast.263
  25.7 0.6 reduce.13
  26.3 0.6 reshape.355
  26.9 0.7 reduce.12
  27.6 0.7 reshape.353
  28.3 4.2 %all-to-all-start.1 = ((bf16[8,2,128]{2,1,0:T(2,128)(2,1)}), bf16[8,2,128]{2,1,0:T(2,128)(2,1)S(1)}, u32[]{:S(2)}, u32[]{:S(2)}) async-start(bf16[8,2,128]{2,1,0:T(2,128)(2,1)} %reshape.355), calls=%async_computation.1 | async-start | bytes 8192 | tf_op jit(solution)/shard_map/all_to_all | solution.py:100
  32.5 0.6 multiply_reduce_fusion.1
  33.9 3.3 %all-to-all-done.1 = bf16[8,2,128]{2,1,0:T(2,128)(2,1)S(1)} async-done(((bf16[8,2,128]{2,1,0:T(2,128)(2,1)}), bf16[8,2,128]{2,1,0:T(2,128)(2,1)S(1)}, u32[]{:S(2)}, u32[]{:S(2)}) %all-to-all-start.1) | async-done | bytes 4128 | tf_op jit(solution)/shard_map/all_to_all | solution.py:100
  37.1 3.3 %all-to-all-start = ((bf16[8,2,2048]{2,1,0:T(2,128)(2,1)}), bf16[8,2,2048]{2,1,0:T(2,128)(2,1)S(1)}, u32[]{:S(2)}, u32[]{:S(2)}) async-start(bf16[8,2,2048]{2,1,0:T(2,128)(2,1)} %reshape.353), calls=%async_computation | async-start | bytes 131072 | tf_op jit(solution)/shard_map/all_to_all | solution.py:99
  40.7 4.8 %all-to-all-done = bf16[8,2,2048]{2,1,0:T(2,128)(2,1)S(1)} async-done(((bf16[8,2,2048]{2,1,0:T(2,128)(2,1)}), bf16[8,2,2048]{2,1,0:T(2,128)(2,1)S(1)}, u32[]{:S(2)}, u32[]{:S(2)}) %all-to-all-start) | async-done | bytes 65568 | tf_op jit(solution)/shard_map/all_to_all | solution.py:99
  45.5 0.4 reduce.7
  46.0 2.5 %fusion.9 = f32[32,1024]{1,0:T(8,128)S(1)} fusion(bf16[32,1024]{1,0:T(8,128)(2,1)S(1)} %reshape.334, bf16[1,1024,1024]{2,1,0:T(8,128)(2,1)} %param.28), kind=kOutput, calls=%fused_computation.14 | convolution fusion | flops 67108864 | bytes 2293760 | tf_op jit(solution)/shard_map/shc,spc->shp/dot_general | solution.py:37
  48.6 0.3 select_reduce_fusion
  48.9 0.2 fusion.79
  49.1 0.2 fusion.45
  49.3 0.5 fusion.15
  49.9 1.0 reduce.14
  50.9 0.7 reshape.357
  51.6 3.3 %all-to-all-start.3 = ((bf16[8,2,2048]{2,1,0:T(2,128)(2,1)}), bf16[8,2,2048]{2,1,0:T(2,128)(2,1)S(1)}, u32[]{:S(2)}, u32[]{:S(2)}) async-start(bf16[8,2,2048]{2,1,0:T(2,128)(2,1)} %reshape.357), calls=%async_computation.3 | async-start | bytes 131072 | tf_op jit(solution)/shard_map/all_to_all | solution.py:126
  55.1 4.8 %all-to-all-done.3 = bf16[8,2,2048]{2,1,0:T(2,128)(2,1)S(1)} async-done(((bf16[8,2,2048]{2,1,0:T(2,128)(2,1)}), bf16[8,2,2048]{2,1,0:T(2,128)(2,1)S(1)}, u32[]{:S(2)}, u32[]{:S(2)}) %all-to-all-start.3) | async-done | bytes 65568 | tf_op jit(solution)/shard_map/all_to_all | solution.py:126
  59.9 0.4 bitcast_reduce_fusion
  60.3 3.7 %convolution_convert_fusion.2 = bf16[8,4096]{1,0:T(8,128)(2,1)} fusion(bf16[512,4096]{1,0:T(8,128)(2,1)} %param.24, bf16[8,4,1024]{2,0,1:T(8,128)(2,1)S(1)} %bitcast.123, bf16[4,1024,128]{2,1,0:T(8,128)(2,1)S(1)} %copy-done.3), kind=kOutput, calls=%fused_computation.6 | convolution fusion | flops 41979904 | bytes 5373952 | tf_op jit(solution)/shard_map/dot_general | solution.py:139
  64.1 52.6 %all-reduce.4.cloned.1.call-done = bf16[8,4096]{1,0:T(8,128)(2,1)} async-done(((bf16[8,4096]{1,0:T(8,128)(2,1)}), bf16[8,4096]{1,0:T(8,128)(2,1)}) %all-reduce.4.cloned.1.call-update) | async-done | bytes 65552 | tf_op jit(solution)/shard_map/psum | solution.py:140
  116.7 1.0 fusion.35
  117.7 1.1 fusion.37
  118.8 0.3 convolution_convert_fusion.1
  119.2 12.5 %all_to_all.77 = bf16[4,7,4096]{2,1,0:T(8,128)(2,1)S(1)} all-to-all(bf16[4,7,4096]{2,1,0:T(8,128)(2,1)S(1)} %all_to_all.64), channel_id=1, replica_groups=mesh['ep'=4,'tp'=8] {'ep'}, dimensions={0} | all-to-all | bytes 458752 | tf_op jit(solution)/shard_map/all_to_all | solution.py:169
  131.8 2.1 fusion.5
  133.9 2.9 %convolution_convert_fusion = bf16[28,4096]{1,0:T(8,128)(2,1)S(1)} fusion(bf16[1,256,4096]{2,1,0:T(8,128)(2,1)S(1)} %copy-done, bf16[28,4096]{1,0:T(8,128)(2,1)S(1)} %all_to_all.66, bf16[1,4096,256]{2,1,0:T(8,128)(2,1)} %param.34, f32[28,256]{1,0:T(8,128)S(1)} %fusion.5), kind=kOutput, calls=%fused_computation | convolution fusion | flops 117598208 | bytes 4681728 | tf_op jit(solution)/shard_map/dot_general | solution.py:173
  136.7 0.8 all_to_all.67
  137.5 3.4 %all-to-all-start.5 = ((bf16[4,7,4096]{2,1,0:T(8,128)(2,1)}), bf16[4,7,4096]{2,1,0:T(8,128)(2,1)S(1)}, u32[]{:S(2)}, u32[]{:S(2)}) async-start(bf16[4,7,4096]{2,1,0:T(8,128)(2,1)} %all_to_all.67), calls=%async_computation.5 | async-start | bytes 524288 | tf_op jit(solution)/shard_map/all_to_all | solution.py:176
  141.1 7.7 %all-to-all-done.5 = bf16[4,7,4096]{2,1,0:T(8,128)(2,1)S(1)} async-done(((bf16[4,7,4096]{2,1,0:T(8,128)(2,1)}), bf16[4,7,4096]{2,1,0:T(8,128)(2,1)S(1)}, u32[]{:S(2)}, u32[]{:S(2)}) %all-to-all-start.5) | async-done | bytes 229408 | tf_op jit(solution)/shard_map/all_to_all | solution.py:176
  149.1 0.8 fusion.1
  149.9 0.6 pad_maximum_fusion.3
  150.4 0.6 dynamic-slice
  151.0 0.6 convert_element_type.184
  151.6 48.9 %all-reduce.6.cloned.1.call-done = bf16[8,4096]{1,0:T(8,128)(2,1)} async-done(((bf16[8,4096]{1,0:T(8,128)(2,1)}), bf16[8,4096]{1,0:T(8,128)(2,1)}) %all-reduce.6.cloned.1.call-update) | async-done | bytes 65552
  200.5 2.0 multiply_reduce_fusion
  203.2 2.1 add_convert_fusion
  (59 shorter events, 2.1 us)
Async XLA Ops:
  7.2 126.7 %copy-start = (bf16[1,256,4096]{2,1,0:T(8,128)(2,1)S(1)}, bf16[1,256,4096]{2,1,0:T(8,128)(2,1)}, u32[]{:S(2)}) copy-start(bf16[1,256,4096]{2,1,0:T(8,128)(2,1)} %param.35) | copy-start | bytes 6291460
  7.2 14.4 %copy-start.7 = (s32[8,2]{0,1:T(2,128)S(1)}, s32[8,2]{0,1:T(2,128)}, u32[]{:S(2)}) copy-start(s32[8,2]{0,1:T(2,128)} %param.31) | copy-start | bytes 196
  7.2 14.8 %copy-start.2 = (bf16[4,128,1024]{2,1,0:T(8,128)(2,1)S(1)}, bf16[4,128,1024]{2,1,0:T(8,128)(2,1)}, u32[]{:S(2)}) copy-start(bf16[4,128,1024]{2,1,0:T(8,128)(2,1)} %param.22) | copy-start | bytes 3145732
  12.3 16.0 %all-to-all-start.2 = ((bf16[8,1,128]{2,1,0:T(2,128)(2,1)}), bf16[8,1,128]{2,1,0:T(2,128)(2,1)S(1)}, u32[]{:S(2)}, u32[]{:S(2)}) async-start(bf16[8,1,128]{2,1,0:T(2,128)(2,1)} %copy.35), calls=%async_computation.2 | async-start | bytes 8192 | tf_op jit(solution)/shard_map/all_to_all | solution.py:101
  22.0 11.8 %copy-start.6 = (f32[1024]{0:T(1024)S(1)}, f32[1024]{0:T(1024)}, u32[]{:S(2)}) copy-start(f32[1024]{0:T(1024)} %param.26) | copy-start | bytes 12292
  25.1 23.4 %copy-start.5 = (bf16[1,1024,64]{1,2,0:T(8,128)(2,1)S(1)}, bf16[1,1024,64]{1,2,0:T(8,128)(2,1)}, u32[]{:S(2)}) copy-start(bf16[1,1024,64]{1,2,0:T(8,128)(2,1)} %param.29) | copy-start | bytes 393220
  28.3 8.8 %all-to-all-start.1 = ((bf16[8,2,128]{2,1,0:T(2,128)(2,1)}), bf16[8,2,128]{2,1,0:T(2,128)(2,1)S(1)}, u32[]{:S(2)}, u32[]{:S(2)}) async-start(bf16[8,2,128]{2,1,0:T(2,128)(2,1)} %reshape.355), calls=%async_computation.1 | async-start | bytes 8192 | tf_op jit(solution)/shard_map/all_to_all | solution.py:100
  37.1 8.3 %all-to-all-start = ((bf16[8,2,2048]{2,1,0:T(2,128)(2,1)}), bf16[8,2,2048]{2,1,0:T(2,128)(2,1)S(1)}, u32[]{:S(2)}, u32[]{:S(2)}) async-start(bf16[8,2,2048]{2,1,0:T(2,128)(2,1)} %reshape.353), calls=%async_computation | async-start | bytes 131072 | tf_op jit(solution)/shard_map/all_to_all | solution.py:99
  45.9 3.4 %copy-start.1 = (bf16[1,1024,1024]{2,1,0:T(8,128)(2,1)S(1)}, bf16[1,1024,1024]{2,1,0:T(8,128)(2,1)}, u32[]{:S(2)}) copy-start(bf16[1,1024,1024]{2,1,0:T(8,128)(2,1)} %param.28) | copy-start | bytes 6291460
  48.4 11.9 %copy-start.3 = (bf16[4,1024,128]{2,1,0:T(8,128)(2,1)S(1)}, bf16[4,1024,128]{2,1,0:T(8,128)(2,1)}, u32[]{:S(2)}) copy-start(bf16[4,1024,128]{2,1,0:T(8,128)(2,1)} %param.23) | copy-start | bytes 3145732
  51.6 8.3 %all-to-all-start.3 = ((bf16[8,2,2048]{2,1,0:T(2,128)(2,1)}), bf16[8,2,2048]{2,1,0:T(2,128)(2,1)S(1)}, u32[]{:S(2)}, u32[]{:S(2)}) async-start(bf16[8,2,2048]{2,1,0:T(2,128)(2,1)} %reshape.357), calls=%async_computation.3 | async-start | bytes 131072 | tf_op jit(solution)/shard_map/all_to_all | solution.py:126
  54.9 61.8 %all-reduce.4.cloned.1.call-start = ((), (), s32[]{:S(2)}) async-start(), calls=%async_computation.6 | async-start | bytes 131072 | tf_op jit(solution)/shard_map/psum | solution.py:140
  60.3 57.4 %copy-start.4 = (bf16[8,4096]{1,0:T(8,128)(2,1)S(1)}, bf16[8,4096]{1,0:T(8,128)(2,1)}, u32[]{:S(2)}) copy-start(bf16[8,4096]{1,0:T(8,128)(2,1)} %param.18) | copy-start | bytes 196612
  133.8 7.1 %copy-start.8 = (f32[8,2]{0,1:T(2,128)S(1)}, f32[8,2]{0,1:T(2,128)}, u32[]{:S(2)}) copy-start(f32[8,2]{0,1:T(2,128)} %param.32) | copy-start | bytes 196
  136.7 13.7 %copy-start.9 = (u32[32]{0:T(128)S(1)}, u32[32]{0:T(128)}, u32[]{:S(2)}) copy-start(u32[32]{0:T(128)} %constant.96) | copy-start | bytes 388
  137.5 11.3 %all-to-all-start.5 = ((bf16[4,7,4096]{2,1,0:T(8,128)(2,1)}), bf16[4,7,4096]{2,1,0:T(8,128)(2,1)S(1)}, u32[]{:S(2)}, u32[]{:S(2)}) async-start(bf16[4,7,4096]{2,1,0:T(8,128)(2,1)} %all_to_all.67), calls=%async_computation.5 | async-start | bytes 524288 | tf_op jit(solution)/shard_map/all_to_all | solution.py:176
  140.9 59.6 %all-reduce.6.cloned.1.call-start = ((), (), s32[]{:S(2)}) async-start(), calls=%async_computation.7 | async-start | bytes 131072
Sparse Core Ops, SparseCore 0:
  64.2 52.5 all-reduce.3
  150.0 50.4 all-reduce.5
where the time goes:
time: 213 us; the launch traced here: 212 us
  waiting for transfers between devices  122 us (57%)
  matrix products  21.2 us (10%)
  starting transfers between devices  19.6 us (9%)
  between operations  16.4 us (8%)
  other arithmetic  12.9 us (6%)
  blocking collectives  12.5 us (6%)
  local copies, waits for them, and re-layouts  7.42 us (3%)
    psum x1, waiting for transfers between devices, on_device(): mixed = lax.psum(head_term.astype(jnp.bfloat16), 'tp').astype(jnp.float32)  52.6 us
    unnamed x3, waiting for transfers between devices  48.9 us
    all_to_all x1, blocking collectives, on_device(): lax.all_to_all(outgoing, 'ep', split_axis=0, concat_axis=0, tiled=True)  12.5 us
    all_to_all x1, waiting for transfers between devices, on_device(): lax.all_to_all(expert_out, 'ep', split_axis=0, concat_axis=0, tiled=True)  7.75 us
    reduce_sum x5, other arithmetic, rms_scale(): jnp.mean(values_f * values_f, axis=-1, keepdims=True) + EPSILON  5.68 us
    all_to_all x1, starting transfers between devices, on_device(): lax.all_to_all(latent_cols, 'tp', split_axis=0, concat_axis=1, tiled=True)  5.2 us
    all_to_all x1, waiting for transfers between devices, on_device(): lax.all_to_all(attended.reshape(seq_count, -1), 'tp', split_axis=1, conca...  4.81 us
    all_to_all x1, waiting for transfers between devices, on_device(): lax.all_to_all(q_latent, 'tp', split_axis=0, concat_axis=1, tiled=True)  4.75 us
  transfers between devices with their start and end apart: 7, of which 6 were waited for; matrix products, arithmetic and copies ran while one was open for 6% of the time, Pallas kernels for 0%

commit v1 on v0

--- a/solution.py
+++ b/solution.py
@@ -137,7 +137,9 @@
         .reshape(group_rows, -1)
     )
     head_term = jnp.dot(values, w_output, preferred_element_type=jnp.float32)
-    mixed = lax.psum(head_term.astype(jnp.bfloat16), "tp").astype(jnp.float32)
+    mixed = jnp.sum(lax.all_gather(head_term.astype(jnp.bfloat16), "tp"), axis=0).astype(
+        jnp.float32
+    )
     resid = (tokens.astype(jnp.float32) + rms_scale(mixed, norm_gains[1])).astype(jnp.bfloat16)
     expert_in = rms_scale(resid, norm_gains[2]).astype(jnp.bfloat16)
     own_resid = lax.dynamic_slice_in_dim(resid, tp_rank * seq_count, seq_count, 0)

time: 213 us -> 170 us (0.80)
  waiting for transfers between devices: 122 us -> 70.3 us
  blocking collectives: 12.5 us -> 22.9 us
    psum x1 -> x0, waiting for transfers between devices: 52.6 us -> none  [on_device(): mixed = lax.psum(head_term.astype(jnp.bfloat16), 'tp').astype(jnp.float32)]
    all_gather x0 -> x1, blocking collectives: none -> 8.88 us  [on_device(): lax.all_gather(head_term.astype(jnp.bfloat16), 'tp')]
    unnamed x3 -> x2, waiting for transfers between devices: 48.9 us -> 49.5 us
  transfers between devices with their start and end apart: 7 -> 6, of which waited for: 6 -> 5; matrix products, arithmetic and copies ran while one was open for 6% -> 8% of each run, Pallas kernels for 0% -> 0%
where the time goes in v1:
time: 170 us; the launch traced here: 169 us
  waiting for transfers between devices  70.3 us (41%)
  blocking collectives  22.9 us (13%)
  matrix products  20.6 us (12%)
  starting transfers between devices  19.5 us (11%)
  between operations  16.4 us (10%)
  other arithmetic  11.4 us (7%)
  local copies, waits for them, and re-layouts  7.42 us (4%)
    unnamed x2, waiting for transfers between devices  49.5 us
    all_to_all x1, blocking collectives, on_device(): lax.all_to_all(outgoing, 'ep', split_axis=0, concat_axis=0, tiled=True)  14.1 us
    all_gather x1, blocking collectives, on_device(): lax.all_gather(head_term.astype(jnp.bfloat16), 'tp')  8.88 us
    all_to_all x1, waiting for transfers between devices, on_device(): lax.all_to_all(expert_out, 'ep', split_axis=0, concat_axis=0, tiled=True)  7.88 us
    all_to_all x1, starting transfers between devices, on_device(): lax.all_to_all(latent_cols, 'tp', split_axis=0, concat_axis=1, tiled=True)  5.2 us
    all_to_all x1, waiting for transfers between devices, on_device(): lax.all_to_all(attended.reshape(seq_count, -1), 'tp', split_axis=1, conca...  4.87 us
    all_to_all x1, waiting for transfers between devices, on_device(): lax.all_to_all(q_latent, 'tp', split_axis=0, concat_axis=1, tiled=True)  4.75 us
    all_to_all x1, starting transfers between devices, on_device(): lax.all_to_all(q_rot, 'tp', split_axis=0, concat_axis=1, tiled=True)  4.2 us
  transfers between devices with their start and end apart: 6, of which 5 were waited for; matrix products, arithmetic and copies ran while one was open for 8% of the time, Pallas kernels for 0%

profile of v1, /device:TPU:0, one launch (start us, length us, event | category | flops | bytes accessed | tf_op | source)
XLA Modules:
  0.0 168.6 jit_solution(14218468985177757310)
XLA Ops:
  7.2 1.1 fusion.78
  8.3 1.1 fusion.40
  9.4 0.9 fusion.42
  10.3 1.5 fusion.29
  11.8 0.6 copy.35
  12.4 5.2 %all-to-all-start.2 = ((bf16[8,1,128]{2,1,0:T(2,128)(2,1)}), bf16[8,1,128]{2,1,0:T(2,128)(2,1)S(1)}, u32[]{:S(2)}, u32[]{:S(2)}) async-start(bf16[8,1,128]{2,1,0:T(2,128)(2,1)} %copy.35), calls=%async_computation.2 | async-start | bytes 8192 | tf_op jit(solution)/shard_map/all_to_all | solution.py:101
  17.6 2.0 %fusion.28 = bf16[8,1,256]{2,0,1:T(8,128)(2,1)S(1)} fusion(bf16[8,4096]{1,0:T(8,128)(2,1)S(1)} %fusion.42, bf16[4096,256]{1,0:T(8,128)(2,1)} %param.21), kind=kOutput, calls=%fused_computation.28 | convolution fusion | flops 16779264 | bytes 2166784 | tf_op jit(solution)/shard_map/dot_general | solution.py:94
  20.3 1.3 fusion.34
  22.0 0.2 select_reduce_fusion.1
  22.2 3.1 %convolution_convert_fusion.3 = bf16[4,8,1024]{2,1,0:T(8,128)(2,1)S(1)} fusion(bf16[4,128,1024]{2,1,0:T(8,128)(2,1)S(1)} %copy-done.2, bf16[8,4096]{1,0:T(8,128)(2,1)S(1)} %fusion.42, bf16[4096,512]{1,0:T(8,128)(2,1)} %param.20), kind=kOutput, calls=%fused_computation.20 | convolution fusion | flops 41979904 | bytes 5373952 | tf_op jit(solution)/shard_map/thn,hnc->thc/dot_general | solution.py:92
  25.3 0.5 broadcast.263
  25.8 0.6 reduce.14
  26.5 0.6 reshape.356
  27.1 0.7 reduce.13
  27.8 0.7 reshape.354
  28.5 4.2 %all-to-all-start.1 = ((bf16[8,2,128]{2,1,0:T(2,128)(2,1)}), bf16[8,2,128]{2,1,0:T(2,128)(2,1)S(1)}, u32[]{:S(2)}, u32[]{:S(2)}) async-start(bf16[8,2,128]{2,1,0:T(2,128)(2,1)} %reshape.356), calls=%async_computation.1 | async-start | bytes 8192 | tf_op jit(solution)/shard_map/all_to_all | solution.py:100
  32.7 0.6 multiply_reduce_fusion.1
  34.1 3.3 %all-to-all-done.1 = bf16[8,2,128]{2,1,0:T(2,128)(2,1)S(1)} async-done(((bf16[8,2,128]{2,1,0:T(2,128)(2,1)}), bf16[8,2,128]{2,1,0:T(2,128)(2,1)S(1)}, u32[]{:S(2)}, u32[]{:S(2)}) %all-to-all-start.1) | async-done | bytes 4128 | tf_op jit(solution)/shard_map/all_to_all | solution.py:100
  37.3 3.3 %all-to-all-start = ((bf16[8,2,2048]{2,1,0:T(2,128)(2,1)}), bf16[8,2,2048]{2,1,0:T(2,128)(2,1)S(1)}, u32[]{:S(2)}, u32[]{:S(2)}) async-start(bf16[8,2,2048]{2,1,0:T(2,128)(2,1)} %reshape.354), calls=%async_computation | async-start | bytes 131072 | tf_op jit(solution)/shard_map/all_to_all | solution.py:99
  40.9 4.8 %all-to-all-done = bf16[8,2,2048]{2,1,0:T(2,128)(2,1)S(1)} async-done(((bf16[8,2,2048]{2,1,0:T(2,128)(2,1)}), bf16[8,2,2048]{2,1,0:T(2,128)(2,1)S(1)}, u32[]{:S(2)}, u32[]{:S(2)}) %all-to-all-start) | async-done | bytes 65568 | tf_op jit(solution)/shard_map/all_to_all | solution.py:99
  45.7 0.4 reduce.8
  46.1 2.5 %fusion.9 = f32[32,1024]{1,0:T(8,128)S(1)} fusion(bf16[32,1024]{1,0:T(8,128)(2,1)S(1)} %reshape.334, bf16[1,1024,1024]{2,1,0:T(8,128)(2,1)} %param.28), kind=kOutput, calls=%fused_computation.14 | convolution fusion | flops 67108864 | bytes 2293760 | tf_op jit(solution)/shard_map/shc,spc->shp/dot_general | solution.py:37
  48.7 0.3 select_reduce_fusion
  49.1 0.2 fusion.79
  49.3 0.2 fusion.45
  49.5 0.5 fusion.15
  50.1 1.0 reduce.15
  51.1 0.7 reshape.358
  51.8 3.3 %all-to-all-start.3 = ((bf16[8,2,2048]{2,1,0:T(2,128)(2,1)}), bf16[8,2,2048]{2,1,0:T(2,128)(2,1)S(1)}, u32[]{:S(2)}, u32[]{:S(2)}) async-start(bf16[8,2,2048]{2,1,0:T(2,128)(2,1)} %reshape.358), calls=%async_computation.3 | async-start | bytes 131072 | tf_op jit(solution)/shard_map/all_to_all | solution.py:126
  55.2 4.9 %all-to-all-done.3 = bf16[8,2,2048]{2,1,0:T(2,128)(2,1)S(1)} async-done(((bf16[8,2,2048]{2,1,0:T(2,128)(2,1)}), bf16[8,2,2048]{2,1,0:T(2,128)(2,1)S(1)}, u32[]{:S(2)}, u32[]{:S(2)}) %all-to-all-start.3) | async-done | bytes 65568 | tf_op jit(solution)/shard_map/all_to_all | solution.py:126
  60.1 0.4 bitcast_reduce_fusion.1
  60.5 3.1 %convolution_convert_fusion.2 = bf16[8,4096]{1,0:T(8,128)(2,1)S(1)} fusion(bf16[512,4096]{1,0:T(8,128)(2,1)} %param.24, bf16[8,4,1024]{2,0,1:T(8,128)(2,1)S(1)} %bitcast.125, bf16[4,1024,128]{2,1,0:T(8,128)(2,1)S(1)} %copy-done.3), kind=kOutput, calls=%fused_computation.6 | convolution fusion | flops 41979904 | bytes 5373952 | tf_op jit(solution)/shard_map/dot_general | solution.py:139
  63.6 8.9 %all-gather = bf16[64,4096]{1,0:T(8,128)(2,1)S(1)} all-gather(bf16[8,4096]{1,0:T(8,128)(2,1)S(1)} %convolution_convert_fusion.2), channel_id=2, replica_groups=mesh['ep'=4,'tp'=8] {'tp'}, dimensions={0}, use_global_device_ids=true | all-gather | bytes 589824 | tf_op jit(solution)/shard_map/all_gather | solution.py:140
  72.7 0.2 fusion.37
  72.9 0.3 convolution_convert_fusion.1
  73.3 14.1 %all_to_all.77 = bf16[4,7,4096]{2,1,0:T(8,128)(2,1)S(1)} all-to-all(bf16[4,7,4096]{2,1,0:T(8,128)(2,1)S(1)} %all_to_all.64), channel_id=1, replica_groups=mesh['ep'=4,'tp'=8] {'ep'}, dimensions={0} | all-to-all | bytes 458752 | tf_op jit(solution)/shard_map/all_to_all | solution.py:171
  87.5 2.1 %fusion.5 = f32[28,256]{1,0:T(8,128)S(1)} fusion(bf16[28,4096]{1,0:T(8,128)(2,1)S(1)} %all_to_all.66, bf16[1,4096,256]{2,1,0:T(8,128)(2,1)} %param.33), kind=kOutput, calls=%fused_computation.10 | convolution fusion | flops 58720256 | bytes 2355200 | tf_op jit(solution)/shard_map/dot_general | solution.py:172
  89.5 2.9 %convolution_convert_fusion = bf16[28,4096]{1,0:T(8,128)(2,1)S(1)} fusion(bf16[1,256,4096]{2,1,0:T(8,128)(2,1)S(1)} %copy-done, bf16[28,4096]{1,0:T(8,128)(2,1)S(1)} %all_to_all.66, bf16[1,4096,256]{2,1,0:T(8,128)(2,1)} %param.34, f32[28,256]{1,0:T(8,128)S(1)} %fusion.5), kind=kOutput, calls=%fused_computation | convolution fusion | flops 117598208 | bytes 4681728 | tf_op jit(solution)/shard_map/dot_general | solution.py:175
  92.4 0.8 all_to_all.67
  93.2 3.4 %all-to-all-start.5 = ((bf16[4,7,4096]{2,1,0:T(8,128)(2,1)}), bf16[4,7,4096]{2,1,0:T(8,128)(2,1)S(1)}, u32[]{:S(2)}, u32[]{:S(2)}) async-start(bf16[4,7,4096]{2,1,0:T(8,128)(2,1)} %all_to_all.67), calls=%async_computation.5 | async-start | bytes 524288 | tf_op jit(solution)/shard_map/all_to_all | solution.py:178
  96.7 7.9 %all-to-all-done.5 = bf16[4,7,4096]{2,1,0:T(8,128)(2,1)S(1)} async-done(((bf16[4,7,4096]{2,1,0:T(8,128)(2,1)}), bf16[4,7,4096]{2,1,0:T(8,128)(2,1)S(1)}, u32[]{:S(2)}, u32[]{:S(2)}) %all-to-all-start.5) | async-done | bytes 229408 | tf_op jit(solution)/shard_map/all_to_all | solution.py:178
  104.9 0.8 fusion.1
  105.7 0.6 pad_maximum_fusion.3
  106.3 0.6 dynamic-slice
  106.8 0.6 convert_element_type.186
  107.4 49.5 %all-reduce.3.cloned.1.call-done = bf16[8,4096]{1,0:T(8,128)(2,1)} async-done(((bf16[8,4096]{1,0:T(8,128)(2,1)}), bf16[8,4096]{1,0:T(8,128)(2,1)}) %all-reduce.3.cloned.1.call-update) | async-done | bytes 65552
  157.0 2.0 %multiply_reduce_fusion = f32[]{:T(128)} fusion(bf16[8,4096]{1,0:T(8,128)(2,1)} %all-reduce.3.cloned.1.call-done, u32[]{:T(128)} %bitcast.36), kind=kLoop, calls=%fused_computation.75 | loop fusion | flops 12287 | bytes 8200 | tf_op jit(solution)/shard_map/reduce_sum | solution.py:15
  159.7 2.1 %add_convert_fusion = bf16[1,4096]{1,0:T(2,128)(2,1)} fusion(f32[4,4096]{1,0:T(4,128)} %param.19, bf16[8,4096]{1,0:T(8,128)(2,1)S(1)} %get-tuple-element.4, s32[]{:T(128)S(6)} %select_n.40, bf16[8,4096]{1,0:T(8,128)(2,1)} %all-reduce.3.cloned.1.call-done, u32[]{:T(128)} %bitcast.36, f32[]{:T(128)S(6)} %rsqrt.36), kind=kLoop, calls=%fused_computation.74 | loop fusion | flops 24576 | bytes 40972 | tf_op jit(solution)/shard_map/convert_element_type | solution.py:186
  (58 shorter events, 2.1 us)
Async XLA Ops:
  7.2 82.3 %copy-start = (bf16[1,256,4096]{2,1,0:T(8,128)(2,1)S(1)}, bf16[1,256,4096]{2,1,0:T(8,128)(2,1)}, u32[]{:S(2)}) copy-start(bf16[1,256,4096]{2,1,0:T(8,128)(2,1)} %param.35) | copy-start | bytes 6291460
  7.2 14.5 %copy-start.7 = (s32[8,2]{0,1:T(2,128)S(1)}, s32[8,2]{0,1:T(2,128)}, u32[]{:S(2)}) copy-start(s32[8,2]{0,1:T(2,128)} %param.31) | copy-start | bytes 196
  8.3 13.9 %copy-start.2 = (bf16[4,128,1024]{2,1,0:T(8,128)(2,1)S(1)}, bf16[4,128,1024]{2,1,0:T(8,128)(2,1)}, u32[]{:S(2)}) copy-start(bf16[4,128,1024]{2,1,0:T(8,128)(2,1)} %param.22) | copy-start | bytes 3145732
  12.4 16.1 %all-to-all-start.2 = ((bf16[8,1,128]{2,1,0:T(2,128)(2,1)}), bf16[8,1,128]{2,1,0:T(2,128)(2,1)S(1)}, u32[]{:S(2)}, u32[]{:S(2)}) async-start(bf16[8,1,128]{2,1,0:T(2,128)(2,1)} %copy.35), calls=%async_computation.2 | async-start | bytes 8192 | tf_op jit(solution)/shard_map/all_to_all | solution.py:101
  22.2 11.8 %copy-start.6 = (f32[1024]{0:T(1024)S(1)}, f32[1024]{0:T(1024)}, u32[]{:S(2)}) copy-start(f32[1024]{0:T(1024)} %param.26) | copy-start | bytes 12292
  25.3 23.4 %copy-start.5 = (bf16[1,1024,64]{1,2,0:T(8,128)(2,1)S(1)}, bf16[1,1024,64]{1,2,0:T(8,128)(2,1)}, u32[]{:S(2)}) copy-start(bf16[1,1024,64]{1,2,0:T(8,128)(2,1)} %param.29) | copy-start | bytes 393220
  28.5 8.8 %all-to-all-start.1 = ((bf16[8,2,128]{2,1,0:T(2,128)(2,1)}), bf16[8,2,128]{2,1,0:T(2,128)(2,1)S(1)}, u32[]{:S(2)}, u32[]{:S(2)}) async-start(bf16[8,2,128]{2,1,0:T(2,128)(2,1)} %reshape.356), calls=%async_computation.1 | async-start | bytes 8192 | tf_op jit(solution)/shard_map/all_to_all | solution.py:100
  37.3 8.3 %all-to-all-start = ((bf16[8,2,2048]{2,1,0:T(2,128)(2,1)}), bf16[8,2,2048]{2,1,0:T(2,128)(2,1)S(1)}, u32[]{:S(2)}, u32[]{:S(2)}) async-start(bf16[8,2,2048]{2,1,0:T(2,128)(2,1)} %reshape.354), calls=%async_computation | async-start | bytes 131072 | tf_op jit(solution)/shard_map/all_to_all | solution.py:99
  46.1 3.4 %copy-start.1 = (bf16[1,1024,1024]{2,1,0:T(8,128)(2,1)S(1)}, bf16[1,1024,1024]{2,1,0:T(8,128)(2,1)}, u32[]{:S(2)}) copy-start(bf16[1,1024,1024]{2,1,0:T(8,128)(2,1)} %param.28) | copy-start | bytes 6291460
  48.6 11.9 %copy-start.3 = (bf16[4,1024,128]{2,1,0:T(8,128)(2,1)S(1)}, bf16[4,1024,128]{2,1,0:T(8,128)(2,1)}, u32[]{:S(2)}) copy-start(bf16[4,1024,128]{2,1,0:T(8,128)(2,1)} %param.23) | copy-start | bytes 3145732
  51.8 8.3 %all-to-all-start.3 = ((bf16[8,2,2048]{2,1,0:T(2,128)(2,1)}), bf16[8,2,2048]{2,1,0:T(2,128)(2,1)S(1)}, u32[]{:S(2)}, u32[]{:S(2)}) async-start(bf16[8,2,2048]{2,1,0:T(2,128)(2,1)} %reshape.358), calls=%async_computation.3 | async-start | bytes 131072 | tf_op jit(solution)/shard_map/all_to_all | solution.py:126
  60.5 12.2 %copy-start.4 = (bf16[8,4096]{1,0:T(8,128)(2,1)S(1)}, bf16[8,4096]{1,0:T(8,128)(2,1)}, u32[]{:S(2)}) copy-start(bf16[8,4096]{1,0:T(8,128)(2,1)} %param.18) | copy-start | bytes 196612
  89.5 7.1 %copy-start.8 = (f32[8,2]{0,1:T(2,128)S(1)}, f32[8,2]{0,1:T(2,128)}, u32[]{:S(2)}) copy-start(f32[8,2]{0,1:T(2,128)} %param.32) | copy-start | bytes 196
  92.4 13.9 %copy-start.9 = (u32[32]{0:T(128)S(1)}, u32[32]{0:T(128)}, u32[]{:S(2)}) copy-start(u32[32]{0:T(128)} %constant.97) | copy-start | bytes 388
  93.2 11.4 %all-to-all-start.5 = ((bf16[4,7,4096]{2,1,0:T(8,128)(2,1)}), bf16[4,7,4096]{2,1,0:T(8,128)(2,1)S(1)}, u32[]{:S(2)}, u32[]{:S(2)}) async-start(bf16[4,7,4096]{2,1,0:T(8,128)(2,1)} %all_to_all.67), calls=%async_computation.5 | async-start | bytes 524288 | tf_op jit(solution)/shard_map/all_to_all | solution.py:178
  96.6 60.4 %all-reduce.3.cloned.1.call-start = ((), (), s32[]{:S(2)}) async-start(), calls=%async_computation.6 | async-start | bytes 131072
Sparse Core Ops, SparseCore 0:
  105.8 51.1 all-reduce.2
